TPU v7x, 32 devices: a whole 2x2x4 slice. The times are simulated.
32 devices in a mesh: ep: 8 (over z, x), tp: 4 (over y, core).
Axes of the slice: x: 2, y: 2, z: 4, core: 2. Of those that a mesh axis runs over, the one named last changes fastest.
Arguments:
- tokens: bfloat16 [1024, 2048], P('ep'), may hold values from -16 to 16
- routes: int32 [1024, 2], P('ep'), may hold values from 0 to 7, all different within a row; in each aligned block of 128 rows (0 to 127, 128 to 255, ...) at most 48 rows name the same one
- router: bfloat16 [2048, 8], replicated, may hold values from -0.125 to 0.125
- w_gate: bfloat16 [8, 2048, 2048], P('ep', None, 'tp'), may hold values from -0.125 to 0.125
- w_up: bfloat16 [8, 2048, 2048], P('ep', None, 'tp'), may hold values from -0.125 to 0.125
- w_down: bfloat16 [8, 2048, 2048], P('ep', 'tp'), may hold values from -0.125 to 0.125
- cotangent: bfloat16 [1024, 2048], P('ep'), may hold values from -6 to 6
Outputs:
- grad_tokens: bfloat16 [1024, 2048], P('ep', 'tp')
- grad_router: float32 [2048, 8], P('tp')
- grad_gate: float32 [8, 2048, 2048], P('ep', None, 'tp')
- grad_up: float32 [8, 2048, 2048], P('ep', None, 'tp')
- grad_down: float32 [8, 2048, 2048], P('ep', 'tp')
Inputs may be any that keep to these rules, and one draw needn't show every extreme that they name: In each aligned block of 128 rows, no expert is named by more than 48 of the block's routes, a bound that some block reaches; a row names 2 different experts.
All inputs are finite; a program needn't handle non-finite values.
Results may differ from a plain program's by a relative error of at most 0.017.
Values may be sent and summed in bfloat16 or wider, within the bound.
No kernel may reach another device: no remote copies, remote signals or barrier semaphores. Data moves between devices by JAX's collectives and lax.ppermute only.
A program may use at most 128 MiB of HBM per device.

v0:
```python
import jax
import jax.numpy as jnp
from jax import lax
from jax.sharding import PartitionSpec as P

clamp_limit = 7.0
sig_slope = 1.702


def on_device(tokens, routes, router, w_gate, w_up, w_down, cotangent):
    highest = lax.Precision.HIGHEST
    ep_count = lax.axis_size("ep")
    tp_count = lax.axis_size("tp")
    tp_index = lax.axis_index("tp")
    tok_rows = tokens.shape[0]
    model_width = tokens.shape[1]
    top_count = routes.shape[1]
    local_experts = w_gate.shape[0]
    all_experts = ep_count * local_experts
    capacity = 3 * tok_rows * top_count // (2 * all_experts)
    slot_count = all_experts * capacity
    feature_part = model_width // tp_count
    feature_start = tp_index * feature_part
    buffer_shape = (ep_count, local_experts, capacity)
    logits = jnp.dot(tokens, router, preferred_element_type=jnp.float32)
    expert_hot = routes[:, :, None] == jnp.arange(all_experts, dtype=jnp.int32)[None, None, :]
    chosen = jnp.sum(jnp.where(expert_hot, logits[:, None, :], 0.0), axis=2)
    weights = 1.0 / jnp.sum(jnp.exp(chosen[:, None, :] - chosen[:, :, None]), axis=2)
    flat_hot = expert_hot.reshape(tok_rows * top_count, all_experts).astype(jnp.int32)
    earlier = jnp.cumsum(flat_hot, axis=0) - flat_hot
    position = jnp.sum(earlier * flat_hot, axis=1).reshape(tok_rows, top_count)
    slot_of = routes * capacity + position
    select = slot_of[None, :, :] == jnp.arange(slot_count, dtype=jnp.int32)[:, None, None]
    dispatch = jnp.any(select, axis=2)
    dispatch_half = dispatch.astype(jnp.bfloat16)
    slot_weight = jnp.sum(jnp.where(select, weights[None, :, :], 0.0), axis=(1, 2))
    token_cols = lax.dynamic_slice_in_dim(tokens, feature_start, feature_part, 1)
    cot_cols = lax.dynamic_slice_in_dim(cotangent, feature_start, feature_part, 1)
    token_slots = jnp.dot(dispatch_half, token_cols, preferred_element_type=jnp.float32).astype(
        jnp.bfloat16
    )
    cot_slots = jnp.dot(dispatch_half, cot_cols, preferred_element_type=jnp.float32).astype(
        jnp.bfloat16
    )
    scaled = (slot_weight[:, None] * cot_slots).astype(jnp.bfloat16)
    sent_tok, sent_cot = (
        lax.all_to_all(
            token_slots.reshape(buffer_shape + (feature_part,)),
            "ep",
            split_axis=0,
            concat_axis=0,
            tiled=True,
        ),
        lax.all_to_all(
            scaled.reshape(buffer_shape + (feature_part,)),
            "ep",
            split_axis=0,
            concat_axis=0,
            tiled=True,
        ),
    )
    arrived, arrived_cot = (
        lax.all_gather(sent_tok, "tp", axis=3, tiled=True),
        lax.all_gather(sent_cot, "tp", axis=3, tiled=True),
    )
    pre_gate = jnp.einsum("slcd,ldf->slcf", arrived, w_gate, preferred_element_type=jnp.float32)
    pre_up = jnp.einsum("slcd,ldf->slcf", arrived, w_up, preferred_element_type=jnp.float32)
    gate_clamped = jnp.minimum(pre_gate, clamp_limit)
    up_clamped = jnp.clip(pre_up, -clamp_limit, clamp_limit)
    sigmoid_gate = jax.nn.sigmoid(sig_slope * gate_clamped)
    gated_act = gate_clamped * sigmoid_gate
    activation = ((up_clamped + 1.0) * gated_act).astype(jnp.bfloat16)
    back_act = jnp.einsum("slcd,lfd->slcf", arrived_cot, w_down, preferred_element_type=jnp.float32)
    share_part = jnp.sum(activation.astype(jnp.float32) * back_act, axis=3)
    slope_term = sigmoid_gate + sig_slope * gated_act * (1.0 - sigmoid_gate)
    d_gate = jnp.where(
        pre_gate < clamp_limit, back_act * (up_clamped + 1.0) * slope_term, 0.0
    ).astype(jnp.bfloat16)
    d_up = jnp.where(jnp.abs(pre_up) < clamp_limit, back_act * gated_act, 0.0).astype(jnp.bfloat16)
    grad_gate = jnp.einsum("slcd,slcf->ldf", arrived, d_gate, preferred_element_type=jnp.float32)
    grad_up = jnp.einsum("slcd,slcf->ldf", arrived, d_up, preferred_element_type=jnp.float32)
    grad_down = jnp.einsum(
        "slcf,slcd->lfd", activation, arrived_cot, preferred_element_type=jnp.float32
    )
    row_term = jnp.einsum("ldf,slcf->dslc", w_gate, d_gate, preferred_element_type=jnp.float32)
    input_part = lax.psum_scatter(
        (
            row_term + jnp.einsum("ldf,slcf->dslc", w_up, d_up, preferred_element_type=jnp.float32)
        ).astype(jnp.bfloat16),
        "tp",
        scatter_dimension=0,
        tiled=True,
    ).astype(jnp.float32)
    share_sum = lax.psum(share_part, "tp")
    back_input, back_share = (
        lax.all_to_all(
            input_part.astype(jnp.bfloat16), "ep", split_axis=1, concat_axis=1, tiled=True
        ).astype(input_part.dtype),
        lax.all_to_all(
            share_sum[None].astype(jnp.bfloat16), "ep", split_axis=1, concat_axis=1, tiled=True
        ).astype(jnp.float32),
    )
    back_input = back_input.reshape(feature_part, slot_count)
    back_share = back_share.reshape(slot_count)
    dispatch_full = dispatch.astype(jnp.float32)
    from_experts = lax.dot_general(
        dispatch_full, back_input, (((0,), (1,)), ((), ())), precision=highest
    )
    shares = jnp.sum(jnp.where(select, back_share[:, None, None], 0.0), axis=0)
    mixed_grad = shares - weights * jnp.sum(shares, axis=1, keepdims=True)
    d_logits = jnp.sum(jnp.where(expert_hot, mixed_grad[:, :, None], 0.0), axis=1)
    router_rows = lax.dynamic_slice_in_dim(router, feature_start, feature_part, 0).astype(
        jnp.float32
    )
    from_router = lax.dot_general(
        d_logits, router_rows, (((1,), (1,)), ((), ())), precision=highest
    )
    grad_tokens = (from_experts + from_router).astype(jnp.bfloat16)
    router_part = lax.dot_general(
        token_cols.astype(jnp.float32), d_logits, (((0,), (0,)), ((), ())), precision=highest
    )
    grad_router = lax.psum(router_part, "ep")
    return (grad_tokens, grad_router, grad_gate, grad_up, grad_down)


def solution(mesh):
    return jax.shard_map(
        on_device,
        mesh=mesh,
        in_specs=(
            P("ep", None),
            P("ep", None),
            P(),
            P("ep", None, "tp"),
            P("ep", None, "tp"),
            P("ep", "tp", None),
            P("ep", None),
        ),
        out_specs=(
            P("ep", "tp"),
            P("tp", None),
            P("ep", None, "tp"),
            P("ep", None, "tp"),
            P("ep", "tp", None),
        ),
        check_vma=False,
    )
```

profile of v0, /device:TPU:0, one launch (start us, length us, event | category | flops | bytes accessed | tf_op | source)
XLA Modules:
  0.0 159.0 jit_solution(8178199809806928618)
XLA Ops:
  7.3 0.9 copy.55
  8.5 0.6 reduce-window.6
  9.1 0.2 slice_reduce_fusion
  9.4 0.1 reshape.140
  9.6 0.7 multiply_add_fusion
  10.4 1.2 convolution_convert_fusion.1
  11.6 19.2 %all_to_all.20 = bf16[8,1,48,512]{3,2,1,0:T(8,128)(2,1)} all-to-all(bf16[8,1,48,512]{3,2,1,0:T(8,128)(2,1)S(1)} %bitcast.163), channel_id=1, replica_groups=mesh['ep'=8,'tp'=4] {'ep'}, dimensions={0} | all-to-all | bytes 786432 | tf_op jit(solution)/shard_map/all_to_all | solution.py:47
  30.9 0.2 fusion.57
  31.2 0.2 select_reduce_fusion.2
  31.4 1.2 fusion.23
  32.5 15.1 %all_to_all.21 = bf16[8,1,48,512]{3,2,1,0:T(8,128)(2,1)} all-to-all(bf16[8,1,48,512]{3,2,1,0:T(8,128)(2,1)S(1)} %bitcast.162), channel_id=1, replica_groups=mesh['ep'=8,'tp'=4] {'ep'}, dimensions={0} | all-to-all | bytes 786432 | tf_op jit(solution)/shard_map/all_to_all | solution.py:54
  47.7 1.6 %all-gather.3.cloned.1.call-done = bf16[8,1,48,2048]{3,2,0,1:T(8,128)(2,1)} async-done(((bf16[8,1,48,512]{3,2,0,1:T(8,128)(2,1)}), bf16[8,1,48,2048]{3,2,0,1:T(8,128)(2,1)}) %all-gather.3.cloned.1.call-update) | async-done | bytes 1572880 | tf_op jit(solution)/shard_map/all_gather | solution.py:63
  49.3 4.0 %fusion.2 = f32[8,48,512]{2,1,0:T(8,128)} fusion(bf16[1,2048,512]{2,1,0:T(8,128)(2,1)} %param.11, bf16[8,1,48,2048]{3,2,0,1:T(8,128)(2,1)} %all-gather.3.cloned.1.call-done), kind=kOutput, calls=%fused_computation.6 | convolution fusion | flops 805306368 | bytes 4456448 | tf_op jit(solution)/shard_map/slcd,ldf->slcf/dot_general | solution.py:67
  53.4 1.9 %fusion.8 = f32[8,48,512]{2,1,0:T(8,128)} fusion(bf16[1,2048,512]{2,1,0:T(8,128)(2,1)S(1)} %copy-done, bf16[8,1,48,2048]{3,2,0,1:T(8,128)(2,1)S(1)} %copy-done.5), kind=kOutput, calls=%fused_computation.12 | convolution fusion | flops 805306368 | bytes 4456448 | tf_op jit(solution)/shard_map/slcd,ldf->slcf/dot_general | solution.py:66
  55.2 15.3 %all-gather.5.cloned.1.call-done = bf16[8,1,48,2048]{3,2,0,1:T(8,128)(2,1)} async-done(((bf16[8,1,48,512]{3,2,0,1:T(8,128)(2,1)}), bf16[8,1,48,2048]{3,2,0,1:T(8,128)(2,1)}) %all-gather.5.cloned.1.call-update) | async-done | bytes 1572880 | tf_op jit(solution)/shard_map/all_gather | solution.py:64
  70.5 4.7 %multiply_reduce_fusion = (f32[8,48]{1,0:T(8,128)S(1)}, bf16[8,1,48,512]{3,2,0,1:T(8,128)(2,1)}, bf16[8,48,512]{2,1,0:T(8,128)(2,1)S(1)}, bf16[8,1,48,512]{3,2,0,1:T(8,128)(2,1)S(1)}) fusion(f32[8,48,512]{2,1,0:T(8,128)} %fusion.8, f32[8,48,512]{2,1,0:T(8,128)} %fusion.2, bf16[1,512,2048]{2,1,0:T(8,128)(2,1)} %param.12, ...), kind=kOutput, calls=%fused_computation.40 | convolution fusion | flops 810614400 | bytes 6424064 | tf_op jit(solution)/shard_map/slcd,lfd->slcf/dot_general | solution.py:73
  75.3 1.0 fusion.6
  76.3 0.5 copy-done.1
  76.9 2.2 %fusion = bf16[2048,8,1,48]{0,3,1,2:T(8,128)(2,1)} fusion(f32[8,48,2048]{2,1,0:T(8,128)S(1)} %fusion.6, bf16[8,48,512]{2,1,0:T(8,128)(2,1)S(1)} %get-tuple-element.9, bf16[1,2048,512]{2,1,0:T(8,128)(2,1)S(1)} %copy-done.1), kind=kOutput, calls=%fused_computation.4 | convolution fusion | flops 806879232 | bytes 7208960 | tf_op jit(solution)/shard_map/ldf,slcf->dslc/dot_general | solution.py:88
  79.1 5.9 %psum.14 = bf16[8,1,48]{2,0,1:T(8,128)(2,1)S(1)} all-reduce(f32[8,1,48]{2,0,1:T(8,128)S(1)} %bitcast.166), channel_id=1, replica_groups=mesh['ep'=8,'tp'=4] {'tp'}, use_global_device_ids=true, to_apply=%region_9.10 | all-reduce | flops 384 | bytes 2304 | tf_op jit(solution)/shard_map/psum | solution.py:94
  85.0 0.6 copy.63
  85.6 5.7 %all-to-all-start.3 = ((bf16[1,8,1,48]{3,2,0,1:T(2,128)(2,1)}), bf16[1,8,1,48]{3,2,0,1:T(2,128)(2,1)S(1)}, u32[]{:S(2)}, u32[]{:S(2)}) async-start(bf16[1,8,1,48]{3,2,0,1:T(2,128)(2,1)} %copy.63), calls=%async_computation.4 | async-start | bytes 8192 | tf_op jit(solution)/shard_map/all_to_all | solution.py:99
  91.3 4.8 %convolution_bitcast_fusion.1 = f32[1,2048,512]{2,1,0:T(8,128)} fusion(bf16[8,48,512]{2,1,0:T(8,128)(2,1)S(1)} %get-tuple-element.9, bf16[8,1,48,2048]{3,2,0,1:T(8,128)(2,1)} %all-gather.3.cloned.1.call-done), kind=kOutput, calls=%fused_computation.1 | convolution fusion | flops 805306368 | bytes 6160384 | tf_op jit(solution)/shard_map/slcd,slcf->ldf/dot_general | solution.py:81
  96.1 3.3 %convolution_bitcast_fusion.2 = f32[1,2048,512]{2,1,0:T(8,128)} fusion(bf16[8,1,48,2048]{3,2,0,1:T(8,128)(2,1)S(1)} %copy-done.6, bf16[8,1,48,512]{3,2,0,1:T(8,128)(2,1)S(1)} %get-tuple-element.10), kind=kOutput, calls=%fused_computation.2 | convolution fusion | flops 805306368 | bytes 6160384 | tf_op jit(solution)/shard_map/slcd,slcf->ldf/dot_general | solution.py:80
  99.5 3.3 %convolution_bitcast_fusion = f32[1,512,2048]{2,1,0:T(8,128)} fusion(bf16[8,1,48,2048]{3,2,0,1:T(8,128)(2,1)S(1)} %copy-done.7, bf16[8,1,48,512]{3,2,0,1:T(8,128)(2,1)S(1)} %copy-done.8), kind=kOutput, calls=%fused_computation | convolution fusion | flops 805306368 | bytes 6160384 | tf_op jit(solution)/shard_map/slcf,slcd->lfd/dot_general | solution.py:82
  102.9 0.2 select_reduce_fusion
  103.1 4.2 %reduce-scatter.2.cloned.1.call-done = bf16[512,8,1,48]{0,3,1,2:T(8,128)(2,1)} async-done(((bf16[2048,8,1,48]{0,3,1,2:T(8,128)(2,1)}), bf16[512,8,1,48]{0,3,1,2:T(8,128)(2,1)}) %reduce-scatter.2.cloned.1.call-update) | async-done | bytes 393232 | tf_op jit(solution)/shard_map/reduce_scatter | solution.py:86
  107.3 5.5 %all-to-all-start.2 = ((bf16[512,8,1,48]{0,3,2,1:T(8,128)(2,1)}), bf16[512,8,1,48]{0,3,2,1:T(8,128)(2,1)S(1)}, u32[]{:S(2)}, u32[]{:S(2)}) async-start(bf16[512,8,1,48]{0,3,2,1:T(8,128)(2,1)} %bitcast.164), calls=%async_computation.3 | async-start | bytes 786432 | tf_op jit(solution)/shard_map/all_to_all | solution.py:96
  112.8 0.2 fusion.40
  113.0 38.3 %psum.15 = f32[512,8]{0,1:T(8,128)} all-reduce(f32[512,8]{0,1:T(8,128)S(1)} %fusion.40), channel_id=1, replica_groups=mesh['ep'=8,'tp'=4] {'ep'}, use_global_device_ids=true, to_apply=%region_13.14 | all-reduce | flops 4096 | bytes 32768 | tf_op jit(solution)/shard_map/psum | solution.py:122
  151.2 0.3 fusion.45
  151.6 0.9 fusion.24
  (40 shorter events, 0.9 us)
Async XLA Ops:
  7.2 46.2 %copy-start = (bf16[1,2048,512]{2,1,0:T(8,128)(2,1)S(1)}, bf16[1,2048,512]{2,1,0:T(8,128)(2,1)}, u32[]{:S(2)}) copy-start(bf16[1,2048,512]{2,1,0:T(8,128)(2,1)} %param.10) | copy-start | bytes 6291460
  7.2 24.0 %copy-start.4 = (s32[128,2]{0,1:T(2,128)S(1)}, s32[128,2]{0,1:T(2,128)}, u32[]{:S(2)}) copy-start(s32[128,2]{0,1:T(2,128)} %param.8) | copy-start | bytes 3076
  7.2 23.7 %copy-start.2 = (bf16[128,2048]{1,0:T(8,128)(2,1)S(1)}, bf16[128,2048]{1,0:T(8,128)(2,1)}, u32[]{:S(2)}) copy-start(bf16[128,2048]{1,0:T(8,128)(2,1)} %param.7) | copy-start | bytes 1572868
  7.2 23.7 %copy-start.3 = (bf16[2048,8]{0,1:T(8,128)(2,1)S(1)}, bf16[2048,8]{0,1:T(8,128)(2,1)}, u32[]{:S(2)}) copy-start(bf16[2048,8]{0,1:T(8,128)(2,1)} %param.9) | copy-start | bytes 98308
  7.2 42.1 %all-gather.3.cloned.1.call-start = ((), (), s32[]{:S(2)}) async-start(), calls=%async_computation.5 | async-start | bytes 1966080 | tf_op jit(solution)/shard_map/all_gather | solution.py:63
  30.8 39.7 %all-gather.5.cloned.1.call-start = ((), (), s32[]{:S(2)}) async-start(), calls=%async_computation.6 | async-start | bytes 1966080 | tf_op jit(solution)/shard_map/all_gather | solution.py:64
  47.6 59.6 %reduce-scatter.2.cloned.1.call-start = ((), (), s32[]{:S(2)}) async-start(), calls=%async_computation.7 | async-start | bytes 1966080 | tf_op jit(solution)/shard_map/reduce_scatter | solution.py:86
  49.3 4.0 %copy-start.5 = (bf16[8,1,48,2048]{3,2,0,1:T(8,128)(2,1)S(1)}, bf16[8,1,48,2048]{3,2,0,1:T(8,128)(2,1)}, u32[]{:S(2)}) copy-start(bf16[8,1,48,2048]{3,2,0,1:T(8,128)(2,1)} %all-gather.3.cloned.1.call-done) | copy-start | bytes 4718596
  75.3 1.6 %copy-start.1 = (bf16[1,2048,512]{2,1,0:T(8,128)(2,1)S(1)}, bf16[1,2048,512]{2,1,0:T(8,128)(2,1)}, u32[]{:S(2)}) copy-start(bf16[1,2048,512]{2,1,0:T(8,128)(2,1)} %param.11) | copy-start | bytes 6291460
  85.6 17.2 %all-to-all-start.3 = ((bf16[1,8,1,48]{3,2,0,1:T(2,128)(2,1)}), bf16[1,8,1,48]{3,2,0,1:T(2,128)(2,1)S(1)}, u32[]{:S(2)}, u32[]{:S(2)}) async-start(bf16[1,8,1,48]{3,2,0,1:T(2,128)(2,1)} %copy.63), calls=%async_computation.4 | async-start | bytes 8192 | tf_op jit(solution)/shard_map/all_to_all | solution.py:99
  91.3 4.9 %copy-start.6 = (bf16[8,1,48,2048]{3,2,0,1:T(8,128)(2,1)S(1)}, bf16[8,1,48,2048]{3,2,0,1:T(8,128)(2,1)}, u32[]{:S(2)}) copy-start(bf16[8,1,48,2048]{3,2,0,1:T(8,128)(2,1)} %all-gather.3.cloned.1.call-done) | copy-start | bytes 4718596
  96.1 3.3 %copy-start.7 = (bf16[8,1,48,2048]{3,2,0,1:T(8,128)(2,1)S(1)}, bf16[8,1,48,2048]{3,2,0,1:T(8,128)(2,1)}, u32[]{:S(2)}) copy-start(bf16[8,1,48,2048]{3,2,0,1:T(8,128)(2,1)} %all-gather.5.cloned.1.call-done) | copy-start | bytes 4718596
  96.1 3.3 %copy-start.8 = (bf16[8,1,48,512]{3,2,0,1:T(8,128)(2,1)S(1)}, bf16[8,1,48,512]{3,2,0,1:T(8,128)(2,1)}, u32[]{:S(2)}) copy-start(bf16[8,1,48,512]{3,2,0,1:T(8,128)(2,1)} %get-tuple-element.8) | copy-start | bytes 1179652
  107.3 44.3 %all-to-all-start.2 = ((bf16[512,8,1,48]{0,3,2,1:T(8,128)(2,1)}), bf16[512,8,1,48]{0,3,2,1:T(8,128)(2,1)S(1)}, u32[]{:S(2)}, u32[]{:S(2)}) async-start(bf16[512,8,1,48]{0,3,2,1:T(8,128)(2,1)} %bitcast.164), calls=%async_computation.3 | async-start | bytes 786432 | tf_op jit(solution)/shard_map/all_to_all | solution.py:96
Sparse Core Ops, SparseCore 0:
  30.9 18.3 all-gather.2
  50.9 19.6 all-gather.4
  79.2 27.9 reduce-scatter.1
where the time goes:
time: 159 us
  blocking collectives  78.5 us (49%)
  matrix products  29.4 us (18%)
  waiting for transfers between devices  21.2 us (13%)
  between operations  13.9 us (9%)
  starting transfers between devices  11.3 us (7%)
  local copies, waits for them, and re-layouts  2.9 us (2%)
  other arithmetic  1.9 us (1%)
    psum x1, blocking collectives, on_device(): grad_router = lax.psum(router_part, 'ep')  38.3 us
    all_to_all x1, blocking collectives, on_device(): lax.all_to_all(token_slots.reshape(buffer_shape + (feature_part,)), 'ep',...  19.2 us
    all_gather x1, waiting for transfers between devices, on_device(): lax.all_gather(sent_cot, 'tp', axis=3, tiled=True)  15.3 us
    all_to_all x1, blocking collectives, on_device(): lax.all_to_all(scaled.reshape(buffer_shape + (feature_part,)), 'ep', spli...  15.1 us
    psum x1, blocking collectives, on_device(): share_sum = lax.psum(share_part, 'tp')  5.89 us
    all_to_all x1, starting transfers between devices, on_device(): lax.all_to_all(share_sum[None].astype(jnp.bfloat16), 'ep', split_axis=1,...  5.67 us
    all_to_all x1, starting transfers between devices, on_device(): lax.all_to_all(input_part.astype(jnp.bfloat16), 'ep', split_axis=1, conca...  5.51 us
    dot_general x1, matrix products, on_device(): jnp.einsum('slcd,slcf->ldf', arrived, d_up, preferred_element_type=jnp.fl...  4.85 us
  transfers between devices with their start and end apart: 5, of which 3 were waited for; matrix products, arithmetic and copies ran while one was open for 13% of the time, Pallas kernels for 0%

commit v1 on v0

--- a/solution.py
+++ b/solution.py
@@ -119,7 +119,11 @@
     router_part = lax.dot_general(
         token_cols.astype(jnp.float32), d_logits, (((0,), (0,)), ((), ())), precision=highest
     )
-    grad_router = lax.psum(router_part, "ep")
+    grad_router = router_part
+    for hop in (1, 2, 4):
+        grad_router = grad_router + lax.ppermute(
+            grad_router, "ep", [(dev, dev ^ hop) for dev in range(8)]
+        )
     return (grad_tokens, grad_router, grad_gate, grad_up, grad_down)
 
 

time: 159 us -> 134 us (0.84)
  blocking collectives: 78.5 us -> 40.2 us
  starting transfers between devices: 11.3 us -> 16.1 us
  waiting for transfers between devices: 21.2 us -> 25.4 us
  matrix products: 29.4 us -> 32 us
    psum x1 -> x0, blocking collectives: 38.3 us -> none  [on_device(): grad_router = lax.psum(router_part, 'ep')]
    ppermute x0 -> x3, starting transfers between devices: none -> 4.84 us  [on_device(): lax.ppermute(grad_router, 'ep', [(dev, dev ^ hop) for dev in range(8)])]
    ppermute x0 -> x3, waiting for transfers between devices: none -> 4.25 us  [on_device(): lax.ppermute(grad_router, 'ep', [(dev, dev ^ hop) for dev in range(8)])]
    reduce_scatter x1, waiting for transfers between devices: 4.19 us -> 2.46 us  [on_device(): lax.psum_scatter((row_term + jnp.einsum('ldf,slcf->dslc', w_up, d_up, pre...]
    all_to_all x1, waiting for transfers between devices: 0.01 us -> 1.69 us  [on_device(): lax.all_to_all(share_sum[None].astype(jnp.bfloat16), 'ep', split_axis=1,...]
  transfers between devices with their start and end apart: 5 -> 8, of which waited for: 3 -> 5; matrix products, arithmetic and copies ran while one was open for 13% -> 18% of each run, Pallas kernels for 0% -> 0%
where the time goes in v1:
time: 134 us; the launch traced here: 133 us
  blocking collectives  40.2 us (30%)
  matrix products  32 us (24%)
  waiting for transfers between devices  25.4 us (19%)
  starting transfers between devices  16.1 us (12%)
  between operations  13.9 us (10%)
  local copies, waits for them, and re-layouts  2.9 us (2%)
  other arithmetic  2.52 us (2%)
    all_to_all x1, blocking collectives, on_device(): lax.all_to_all(token_slots.reshape(buffer_shape + (feature_part,)), 'ep',...  19.2 us
    all_gather x1, waiting for transfers between devices, on_device(): lax.all_gather(sent_cot, 'tp', axis=3, tiled=True)  15.3 us
    all_to_all x1, blocking collectives, on_device(): lax.all_to_all(scaled.reshape(buffer_shape + (feature_part,)), 'ep', spli...  15.1 us
    psum x1, blocking collectives, on_device(): share_sum = lax.psum(share_part, 'tp')  5.89 us
    all_to_all x1, starting transfers between devices, on_device(): lax.all_to_all(share_sum[None].astype(jnp.bfloat16), 'ep', split_axis=1,...  5.67 us
    all_to_all x1, starting transfers between devices, on_device(): lax.all_to_all(input_part.astype(jnp.bfloat16), 'ep', split_axis=1, conca...  5.51 us
    ppermute x3, starting transfers between devices, on_device(): lax.ppermute(grad_router, 'ep', [(dev, dev ^ hop) for dev in range(8)])  4.84 us
    dot_general x1, matrix products, on_device(): jnp.einsum('slcd,slcf->ldf', arrived, d_up, preferred_element_type=jnp.fl...  4.73 us
  transfers between devices with their start and end apart: 8, of which 5 were waited for; matrix products, arithmetic and copies ran while one was open for 18% of the time, Pallas kernels for 0%

profile of v1, /device:TPU:0, one launch (start us, length us, event | category | flops | bytes accessed | tf_op | source)
XLA Modules:
  0.0 133.0 jit_solution(7362965377217353769)
XLA Ops:
  7.3 0.9 copy.55
  8.5 0.6 reduce-window.6
  9.6 0.7 multiply_add_fusion
  10.4 1.2 convolution_convert_fusion.1
  11.6 19.2 %all_to_all.20 = bf16[8,1,48,512]{3,2,1,0:T(8,128)(2,1)} all-to-all(bf16[8,1,48,512]{3,2,1,0:T(8,128)(2,1)S(1)} %bitcast.163), channel_id=1, replica_groups=mesh['ep'=8,'tp'=4] {'ep'}, dimensions={0} | all-to-all | bytes 786432 | tf_op jit(solution)/shard_map/all_to_all | solution.py:47
  30.9 0.2 fusion.57
  31.4 1.2 fusion.23
  32.5 15.1 %all_to_all.21 = bf16[8,1,48,512]{3,2,1,0:T(8,128)(2,1)} all-to-all(bf16[8,1,48,512]{3,2,1,0:T(8,128)(2,1)S(1)} %bitcast.162), channel_id=1, replica_groups=mesh['ep'=8,'tp'=4] {'ep'}, dimensions={0} | all-to-all | bytes 786432 | tf_op jit(solution)/shard_map/all_to_all | solution.py:54
  47.7 1.6 %all-gather.3.cloned.1.call-done = bf16[8,1,48,2048]{3,2,0,1:T(8,128)(2,1)} async-done(((bf16[8,1,48,512]{3,2,0,1:T(8,128)(2,1)}), bf16[8,1,48,2048]{3,2,0,1:T(8,128)(2,1)}) %all-gather.3.cloned.1.call-update) | async-done | bytes 1572880 | tf_op jit(solution)/shard_map/all_gather | solution.py:63
  49.3 4.0 %fusion.2 = f32[8,48,512]{2,1,0:T(8,128)} fusion(bf16[1,2048,512]{2,1,0:T(8,128)(2,1)} %param.11, bf16[8,1,48,2048]{3,2,0,1:T(8,128)(2,1)} %all-gather.3.cloned.1.call-done), kind=kOutput, calls=%fused_computation.6 | convolution fusion | flops 805306368 | bytes 4456448 | tf_op jit(solution)/shard_map/slcd,ldf->slcf/dot_general | solution.py:67
  53.4 1.9 %fusion.8 = f32[8,48,512]{2,1,0:T(8,128)} fusion(bf16[1,2048,512]{2,1,0:T(8,128)(2,1)S(1)} %copy-done, bf16[8,1,48,2048]{3,2,0,1:T(8,128)(2,1)S(1)} %copy-done.5), kind=kOutput, calls=%fused_computation.12 | convolution fusion | flops 805306368 | bytes 4456448 | tf_op jit(solution)/shard_map/slcd,ldf->slcf/dot_general | solution.py:66
  55.2 15.3 %all-gather.5.cloned.1.call-done = bf16[8,1,48,2048]{3,2,0,1:T(8,128)(2,1)} async-done(((bf16[8,1,48,512]{3,2,0,1:T(8,128)(2,1)}), bf16[8,1,48,2048]{3,2,0,1:T(8,128)(2,1)}) %all-gather.5.cloned.1.call-update) | async-done | bytes 1572880 | tf_op jit(solution)/shard_map/all_gather | solution.py:64
  70.6 4.7 %multiply_reduce_fusion = (f32[8,48]{1,0:T(8,128)S(1)}, bf16[8,1,48,512]{3,2,0,1:T(8,128)(2,1)}, bf16[8,48,512]{2,1,0:T(8,128)(2,1)S(1)}, bf16[8,1,48,512]{3,2,0,1:T(8,128)(2,1)S(1)}) fusion(f32[8,48,512]{2,1,0:T(8,128)} %fusion.8, f32[8,48,512]{2,1,0:T(8,128)} %fusion.2, bf16[1,512,2048]{2,1,0:T(8,128)(2,1)} %param.12, ...), kind=kOutput, calls=%fused_computation.40 | convolution fusion | flops 810614400 | bytes 6424064 | tf_op jit(solution)/shard_map/slcd,lfd->slcf/dot_general | solution.py:73
  75.3 1.0 fusion.6
  76.3 0.6 copy-done.1
  76.9 2.2 %fusion = bf16[2048,8,1,48]{0,3,1,2:T(8,128)(2,1)} fusion(f32[8,48,2048]{2,1,0:T(8,128)S(1)} %fusion.6, bf16[8,48,512]{2,1,0:T(8,128)(2,1)S(1)} %get-tuple-element.9, bf16[1,2048,512]{2,1,0:T(8,128)(2,1)S(1)} %copy-done.1), kind=kOutput, calls=%fused_computation.4 | convolution fusion | flops 806879232 | bytes 7208960 | tf_op jit(solution)/shard_map/ldf,slcf->dslc/dot_general | solution.py:88
  79.1 5.9 %psum.7 = bf16[8,1,48]{2,0,1:T(8,128)(2,1)S(1)} all-reduce(f32[8,1,48]{2,0,1:T(8,128)S(1)} %bitcast.166), channel_id=1, replica_groups=mesh['ep'=8,'tp'=4] {'tp'}, use_global_device_ids=true, to_apply=%region_9.10 | all-reduce | flops 384 | bytes 2304 | tf_op jit(solution)/shard_map/psum | solution.py:94
  84.9 0.6 copy.63
  85.5 5.7 %all-to-all-start.3 = ((bf16[1,8,1,48]{3,2,0,1:T(2,128)(2,1)}), bf16[1,8,1,48]{3,2,0,1:T(2,128)(2,1)S(1)}, u32[]{:S(2)}, u32[]{:S(2)}) async-start(bf16[1,8,1,48]{3,2,0,1:T(2,128)(2,1)} %copy.63), calls=%async_computation.4 | async-start | bytes 8192 | tf_op jit(solution)/shard_map/all_to_all | solution.py:99
  91.2 4.7 %convolution_bitcast_fusion.1 = f32[1,2048,512]{2,1,0:T(8,128)} fusion(bf16[8,48,512]{2,1,0:T(8,128)(2,1)S(1)} %get-tuple-element.9, bf16[8,1,48,2048]{3,2,0,1:T(8,128)(2,1)} %all-gather.3.cloned.1.call-done), kind=kOutput, calls=%fused_computation.1 | convolution fusion | flops 805306368 | bytes 6160384 | tf_op jit(solution)/shard_map/slcd,slcf->ldf/dot_general | solution.py:81
  95.9 1.7 %all-to-all-done.3 = bf16[1,8,1,48]{3,2,0,1:T(2,128)(2,1)S(1)} async-done(((bf16[1,8,1,48]{3,2,0,1:T(2,128)(2,1)}), bf16[1,8,1,48]{3,2,0,1:T(2,128)(2,1)S(1)}, u32[]{:S(2)}, u32[]{:S(2)}) %all-to-all-start.3) | async-done | bytes 800 | tf_op jit(solution)/shard_map/all_to_all | solution.py:99
  98.1 0.6 collective-permute-start
  98.7 4.7 %convolution_bitcast_fusion.2 = f32[1,2048,512]{2,1,0:T(8,128)} fusion(bf16[8,1,48,2048]{3,2,0,1:T(8,128)(2,1)} %all-gather.3.cloned.1.call-done, bf16[8,1,48,512]{3,2,0,1:T(8,128)(2,1)S(1)} %get-tuple-element.10), kind=kOutput, calls=%fused_computation.2 | convolution fusion | flops 805306368 | bytes 6160384 | tf_op jit(solution)/shard_map/slcd,slcf->ldf/dot_general | solution.py:80
  103.4 1.3 collective-permute-start.1
  104.7 2.5 %reduce-scatter.2.cloned.1.call-done = bf16[512,8,1,48]{0,3,1,2:T(8,128)(2,1)} async-done(((bf16[2048,8,1,48]{0,3,1,2:T(8,128)(2,1)}), bf16[512,8,1,48]{0,3,1,2:T(8,128)(2,1)}) %reduce-scatter.2.cloned.1.call-update) | async-done | bytes 393232 | tf_op jit(solution)/shard_map/reduce_scatter | solution.py:86
  107.2 5.5 %all-to-all-start.2 = ((bf16[512,8,1,48]{0,3,2,1:T(8,128)(2,1)}), bf16[512,8,1,48]{0,3,2,1:T(8,128)(2,1)S(1)}, u32[]{:S(2)}, u32[]{:S(2)}) async-start(bf16[512,8,1,48]{0,3,2,1:T(8,128)(2,1)} %bitcast.164), calls=%async_computation.3 | async-start | bytes 786432 | tf_op jit(solution)/shard_map/all_to_all | solution.py:96
  112.7 4.7 %convolution_bitcast_fusion = f32[1,512,2048]{2,1,0:T(8,128)} fusion(bf16[8,1,48,2048]{3,2,0,1:T(8,128)(2,1)} %all-gather.5.cloned.1.call-done, bf16[8,1,48,512]{3,2,0,1:T(8,128)(2,1)S(1)} %copy-done.6), kind=kOutput, calls=%fused_computation | convolution fusion | flops 805306368 | bytes 6160384 | tf_op jit(solution)/shard_map/slcf,slcd->lfd/dot_general | solution.py:82
  117.4 3.0 %collective-permute-start.2 = (f32[512,8]{0,1:T(8,128)S(1)}, f32[512,8]{0,1:T(8,128)S(1)}, u32[]{:S(2)}, u32[]{:S(2)}) collective-permute-start(f32[512,8]{0,1:T(8,128)S(1)} %add.59), channel_id=1, source_target_pairs={{0,16},{4,20},{8,24},{12,28},{16,0},{20,4},{24,8},{28,12},{1,17},{... | collective-permute-start | bytes 49160 | tf_op jit(solution)/shard_map/ppermute | solution.py:124
  120.4 0.3 fusion.45
  120.7 4.2 %collective-permute-done.2 = f32[512,8]{0,1:T(8,128)S(1)} collective-permute-done((f32[512,8]{0,1:T(8,128)S(1)}, f32[512,8]{0,1:T(8,128)S(1)}, u32[]{:S(2)}, u32[]{:S(2)}) %collective-permute-start.2) | collective-permute-done | bytes 16416 | tf_op jit(solution)/shard_map/ppermute | solution.py:124
  125.0 0.6 add.60
  125.6 0.9 fusion.24
  (44 shorter events, 1.8 us)
Async XLA Ops:
  7.2 46.2 %copy-start = (bf16[1,2048,512]{2,1,0:T(8,128)(2,1)S(1)}, bf16[1,2048,512]{2,1,0:T(8,128)(2,1)}, u32[]{:S(2)}) copy-start(bf16[1,2048,512]{2,1,0:T(8,128)(2,1)} %param.10) | copy-start | bytes 6291460
  7.2 24.0 %copy-start.4 = (s32[128,2]{0,1:T(2,128)S(1)}, s32[128,2]{0,1:T(2,128)}, u32[]{:S(2)}) copy-start(s32[128,2]{0,1:T(2,128)} %param.8) | copy-start | bytes 3076
  7.2 23.7 %copy-start.2 = (bf16[128,2048]{1,0:T(8,128)(2,1)S(1)}, bf16[128,2048]{1,0:T(8,128)(2,1)}, u32[]{:S(2)}) copy-start(bf16[128,2048]{1,0:T(8,128)(2,1)} %param.7) | copy-start | bytes 1572868
  7.2 23.7 %copy-start.3 = (bf16[2048,8]{0,1:T(8,128)(2,1)S(1)}, bf16[2048,8]{0,1:T(8,128)(2,1)}, u32[]{:S(2)}) copy-start(bf16[2048,8]{0,1:T(8,128)(2,1)} %param.9) | copy-start | bytes 98308
  7.2 42.1 %all-gather.3.cloned.1.call-start = ((), (), s32[]{:S(2)}) async-start(), calls=%async_computation.5 | async-start | bytes 1966080 | tf_op jit(solution)/shard_map/all_gather | solution.py:63
  30.8 39.7 %all-gather.5.cloned.1.call-start = ((), (), s32[]{:S(2)}) async-start(), calls=%async_computation.6 | async-start | bytes 1966080 | tf_op jit(solution)/shard_map/all_gather | solution.py:64
  47.6 59.5 %reduce-scatter.2.cloned.1.call-start = ((), (), s32[]{:S(2)}) async-start(), calls=%async_computation.7 | async-start | bytes 1966080 | tf_op jit(solution)/shard_map/reduce_scatter | solution.py:86
  49.3 4.0 %copy-start.5 = (bf16[8,1,48,2048]{3,2,0,1:T(8,128)(2,1)S(1)}, bf16[8,1,48,2048]{3,2,0,1:T(8,128)(2,1)}, u32[]{:S(2)}) copy-start(bf16[8,1,48,2048]{3,2,0,1:T(8,128)(2,1)} %all-gather.3.cloned.1.call-done) | copy-start | bytes 4718596
  75.3 1.6 %copy-start.1 = (bf16[1,2048,512]{2,1,0:T(8,128)(2,1)S(1)}, bf16[1,2048,512]{2,1,0:T(8,128)(2,1)}, u32[]{:S(2)}) copy-start(bf16[1,2048,512]{2,1,0:T(8,128)(2,1)} %param.11) | copy-start | bytes 6291460
  85.5 12.1 %all-to-all-start.3 = ((bf16[1,8,1,48]{3,2,0,1:T(2,128)(2,1)}), bf16[1,8,1,48]{3,2,0,1:T(2,128)(2,1)S(1)}, u32[]{:S(2)}, u32[]{:S(2)}) async-start(bf16[1,8,1,48]{3,2,0,1:T(2,128)(2,1)} %copy.63), calls=%async_computation.4 | async-start | bytes 8192 | tf_op jit(solution)/shard_map/all_to_all | solution.py:99
  98.1 14.6 %copy-start.6 = (bf16[8,1,48,512]{3,2,0,1:T(8,128)(2,1)S(1)}, bf16[8,1,48,512]{3,2,0,1:T(8,128)(2,1)}, u32[]{:S(2)}) copy-start(bf16[8,1,48,512]{3,2,0,1:T(8,128)(2,1)} %get-tuple-element.8) | copy-start | bytes 1179652
  98.1 5.3 %collective-permute-start = (f32[512,8]{0,1:T(8,128)S(1)}, f32[512,8]{0,1:T(8,128)S(1)}, u32[]{:S(2)}, u32[]{:S(2)}) collective-permute-start(f32[512,8]{0,1:T(8,128)S(1)} %fusion.40), channel_id=1, source_target_pairs={{0,4},{4,0},{8,12},{12,8},{16,20},{20,16},{24,28},{28,24},{1,5},{5... | collective-permute-start | bytes 49160 | tf_op jit(solution)/shard_map/ppermute | solution.py:124
  103.4 14.0 %collective-permute-start.1 = (f32[512,8]{0,1:T(8,128)S(1)}, f32[512,8]{0,1:T(8,128)S(1)}, u32[]{:S(2)}, u32[]{:S(2)}) collective-permute-start(f32[512,8]{0,1:T(8,128)S(1)} %add.58), channel_id=1, source_target_pairs={{0,8},{4,12},{8,0},{12,4},{16,24},{20,28},{24,16},{28,20},{1,9},{5... | collective-permute-start | bytes 49160 | tf_op jit(solution)/shard_map/ppermute | solution.py:124
  107.2 18.4 %all-to-all-start.2 = ((bf16[512,8,1,48]{0,3,2,1:T(8,128)(2,1)}), bf16[512,8,1,48]{0,3,2,1:T(8,128)(2,1)S(1)}, u32[]{:S(2)}, u32[]{:S(2)}) async-start(bf16[512,8,1,48]{0,3,2,1:T(8,128)(2,1)} %bitcast.164), calls=%async_computation.3 | async-start | bytes 786432 | tf_op jit(solution)/shard_map/all_to_all | solution.py:96
  117.4 7.5 %collective-permute-start.2 = (f32[512,8]{0,1:T(8,128)S(1)}, f32[512,8]{0,1:T(8,128)S(1)}, u32[]{:S(2)}, u32[]{:S(2)}) collective-permute-start(f32[512,8]{0,1:T(8,128)S(1)} %add.59), channel_id=1, source_target_pairs={{0,16},{4,20},{8,24},{12,28},{16,0},{20,4},{24,8},{28,12},{1,17},{... | collective-permute-start | bytes 49160 | tf_op jit(solution)/shard_map/ppermute | solution.py:124
Sparse Core Ops, SparseCore 0:
  31.0 18.3 all-gather.2
  50.9 19.6 all-gather.4
  79.2 27.9 reduce-scatter.1
